TPU v7x, 32 devices: a whole 2x2x4 slice. The times are simulated.
32 devices in a mesh: ep: 8 (over z, y), tp: 4 (over x, core).
Axes of the slice: x: 2, y: 2, z: 4, core: 2. Of those that a mesh axis runs over, the one named last changes fastest.
Arguments:
- tokens: bfloat16 [2048, 2048], P('ep'), may hold values from -6 to 6
- norm_gain: float32 [2048], replicated, may hold values from 0.1 to 1.9
- expert_ids: int32 [2048, 2], P('ep'), may hold values from 0 to 3, all different within a row; in each aligned block of 256 rows (0 to 255, 256 to 511, ...) at most 160 rows name the same one
- route_weight: float32 [2048, 2], P('ep'), may hold values from 0.2 to 1
- w_gate: bfloat16 [8, 2048, 3584], P('ep', None, 'tp'), may hold values from -0.125 to 0.125
- w_up: bfloat16 [8, 2048, 3584], P('ep', None, 'tp'), may hold values from -0.125 to 0.125
- w_down: bfloat16 [8, 3584, 2048], P('ep', 'tp'), may hold values from -0.0625 to 0.0625
Outputs:
- mixed: bfloat16 [2048, 2048], P('ep', 'tp')
Inputs may be any that keep to these rules, and one draw needn't show every extreme that they name: `expert_ids`: A token names 2 different experts. In each aligned block of 256 tokens (the tokens of one index of ep) no expert is named by more than 160 tokens, a bound that some block reaches.
All inputs are finite; a program needn't handle non-finite values.
Results may differ from a plain program's by a relative error of at most 0.014.
Values may be sent and summed in bfloat16 or wider, within the bound.
A program may use at most 128 MiB of HBM per device.

v0:
```python
import jax
import jax.numpy as jnp
from jax import lax
from jax.sharding import PartitionSpec as P

HALVES = 2
EPSILON = 1e-05


def layer_normed(tokens, norm_gain):
    values = tokens.astype(jnp.float32)
    center = values - jnp.mean(values, axis=-1, keepdims=True)
    spread = jnp.mean(center * center, axis=-1, keepdims=True)
    return (center * lax.rsqrt(spread + EPSILON) * norm_gain).astype(jnp.bfloat16)


def slot_numbers(chosen, experts):
    onehot = (chosen[..., None] == jnp.arange(experts, dtype=jnp.int32)).astype(jnp.int32)
    before = jnp.cumsum(onehot, axis=1) - onehot
    return jnp.sum(before * onehot, axis=-1)


def body(tokens, norm_gain, expert_ids, route_weight, w_gate, w_up, w_down):
    tok_rows, width = tokens.shape
    top_count = expert_ids.shape[1]
    ep_count = lax.axis_size("ep")
    experts = ep_count // HALVES
    capacity = 2 * min(tok_rows // 2, 5 * tok_rows * top_count // (8 * experts))
    normed = layer_normed(tokens, norm_gain)
    padded = jnp.concatenate([normed, jnp.zeros((1, width), jnp.bfloat16)], axis=0)
    slots = slot_numbers(expert_ids.reshape(1, -1), experts).reshape(-1)
    flat_expert = expert_ids.reshape(-1)
    owner = jnp.arange(tok_rows * top_count, dtype=jnp.int32) // top_count
    place = flat_expert * capacity + slots
    table = jnp.full((experts * capacity,), tok_rows, jnp.int32).at[place].set(owner)
    outgoing = padded[table].reshape(experts, capacity, width)
    columns = width // lax.axis_size("tp")
    portion = lax.dynamic_slice_in_dim(outgoing, lax.axis_index("tp") * columns, columns, 2)
    doubled = jnp.repeat(portion, HALVES, axis=0)
    pieces = lax.all_to_all(doubled, "ep", split_axis=0, concat_axis=0, tiled=True)
    arrived = lax.all_gather(pieces, "tp", axis=2, tiled=True)
    routed = arrived.reshape(-1, width)
    gate = jnp.dot(routed, w_gate[0], preferred_element_type=jnp.float32)
    up = jnp.dot(routed, w_up[0], preferred_element_type=jnp.float32)
    hidden = (jax.nn.silu(gate) * up).astype(jnp.bfloat16)
    partial_value = jnp.dot(hidden, w_down[0], preferred_element_type=jnp.float32)
    reduced = lax.psum_scatter(
        partial_value.astype(jnp.bfloat16), "tp", scatter_dimension=1, tiled=True
    )
    returned = lax.all_to_all(
        reduced.reshape(ep_count, capacity, -1), "ep", split_axis=0, concat_axis=0, tiled=True
    )
    quarter = returned.shape[2]
    summed = returned.reshape(experts, HALVES, capacity, quarter).astype(jnp.float32).sum(axis=1)
    picked = summed.reshape(experts * capacity, quarter)[place].reshape(
        tok_rows, top_count, quarter
    )
    mixed = jnp.sum(route_weight[:, :, None] * picked, axis=1)
    return mixed.astype(jnp.bfloat16)


def solution(mesh):
    return jax.shard_map(
        body,
        mesh=mesh,
        in_specs=(
            P("ep", None),
            P(),
            P("ep", None),
            P("ep", None),
            P("ep", None, "tp"),
            P("ep", None, "tp"),
            P("ep", "tp", None),
        ),
        out_specs=P("ep", "tp"),
        check_vma=False,
    )
```

profile of v0, /device:TPU:0, one launch (start us, length us, event | category | flops | bytes accessed | tf_op | source)
XLA Modules:
  0.0 228.1 jit_solution(8858825932461723816)
XLA Ops:
  6.5 0.8 copy.11
  7.4 0.1 eq.27
  7.5 1.2 reduce-window.6
  8.8 0.2 slice_reduce_fusion
  9.0 0.7 broadcast_multiply_fusion
  9.7 0.2 reduce-window.9
  9.9 0.1 broadcast.113
  10.0 0.1 copy.10
  10.1 0.1 mul.64
  10.3 2.4 %scatter_custom_fusion = s32[640]{0:T(1024)S(1)} fusion(s32[512]{0:T(512)S(1)} %bitcast.41, s32[512]{0:T(512)S(1)} %add_select_fusion, s32[]{:T(128)} %constant.41.clone.1), kind=kCustom, calls=%fused_computation.35 | custom fusion | bytes 2564 | tf_op jit(solution)/shard_map/scatter | solution.py:35
  12.8 1.4 convert_reduce_fusion
  14.2 1.6 fusion.6
  15.9 1.6 fusion.8
  17.5 0.1 concatenate.3
  17.6 4.1 %gather_fusion = bf16[640,2048]{1,0:T(8,128)(2,1)} fusion(bf16[257,2048]{1,0:T(8,128)(2,1)S(1)} %concatenate.3, s32[1024]{0:T(1024)S(1)} %pad_clamp_fusion.1), kind=kCustom, calls=%fused_computation | custom fusion | bytes 5245440 | tf_op jit(solution)/shard_map/gather | solution.py:36
  21.7 1.1 constant_dynamic-slice_fusion
  22.8 0.1 broadcast_in_dim.8
  22.9 38.6 %all_to_all.10 = bf16[8,160,512]{2,1,0:T(8,128)(2,1)} all-to-all(bf16[8,160,512]{2,1,0:T(8,128)(2,1)S(1)} %bitcast.38), channel_id=1, replica_groups=mesh['ep'=8,'tp'=4] {'ep'}, dimensions={0} | all-to-all | bytes 2621440 | tf_op jit(solution)/shard_map/all_to_all | solution.py:40
  61.5 0.0 all-gather.2.cloned.1.call-update
  61.5 0.0 reduce-scatter.2.cloned.1.call-start
  61.6 39.5 %all-gather.2.cloned.1.call-done = bf16[8,160,2048]{2,1,0:T(8,128)(2,1)} async-done(((bf16[8,160,512]{2,1,0:T(8,128)(2,1)}), bf16[8,160,2048]{2,1,0:T(8,128)(2,1)}) %all-gather.2.cloned.1.call-update) | async-done | bytes 5242896 | tf_op jit(solution)/shard_map/all_gather | solution.py:41
  101.1 10.0 %fusion.2 = f32[1280,896]{1,0:T(8,128)} fusion(bf16[1280,2048]{1,0:T(8,128)(2,1)} %bitcast.45, bf16[1,2048,896]{2,1,0:T(8,128)(2,1)} %param.11), kind=kOutput, calls=%fused_computation.7 | convolution fusion | flops 4697620480 | bytes 13500416 | tf_op jit(solution)/shard_map/dot_general | solution.py:43
  111.1 17.6 %convolution_convert_fusion = bf16[1280,2048]{1,0:T(8,128)(2,1)} fusion(bf16[1,896,2048]{2,1,0:T(8,128)(2,1)} %param.13, f32[1280,896]{1,0:T(8,128)} %fusion.2, bf16[1280,2048]{1,0:T(8,128)(2,1)} %bitcast.46, bf16[1,2048,896]{2,1,0:T(8,128)(2,1)} %param.12), kind=kOutput, calls=%fused_computation.3 | convolution fusion | flops 9404743680 | bytes 22413312 | tf_op jit(solution)/shard_map/dot_general | solution.py:46
  128.6 0.0 reduce-scatter.2.cloned.1.call-update
  128.7 51.3 %reduce-scatter.2.cloned.1.call-done = bf16[1280,512]{1,0:T(8,128)(2,1)} async-done(((bf16[1280,2048]{1,0:T(8,128)(2,1)}), bf16[1280,512]{1,0:T(8,128)(2,1)}) %reduce-scatter.2.cloned.1.call-update) | async-done | bytes 1310736 | tf_op jit(solution)/shard_map/reduce_scatter | solution.py:47
  180.0 5.5 %all-to-all-start.1 = ((bf16[8,160,512]{2,1,0:T(8,128)(2,1)}), bf16[8,160,512]{2,1,0:T(8,128)(2,1)S(1)}, u32[]{:S(2)}, u32[]{:S(2)}) async-start(bf16[8,160,512]{2,1,0:T(8,128)(2,1)} %bitcast.40), calls=%async_computation.2 | async-start | bytes 2621440 | tf_op jit(solution)/shard_map/all_to_all | solution.py:50
  185.5 0.1 copy.9
  185.7 31.1 %all-to-all-done.1 = bf16[8,160,512]{2,1,0:T(8,128)(2,1)S(1)} async-done(((bf16[8,160,512]{2,1,0:T(8,128)(2,1)}), bf16[8,160,512]{2,1,0:T(8,128)(2,1)S(1)}, u32[]{:S(2)}, u32[]{:S(2)}) %all-to-all-start.1) | async-done | bytes 1310752 | tf_op jit(solution)/shard_map/all_to_all | solution.py:50
  216.7 0.2 convert_reduce_fusion.1
  216.9 1.6 gather_fusion.1
  218.6 0.6 reshape.191
  219.2 2.1 multiply_reduce_fusion
  (16 shorter events, 0.1 us)
Async XLA Ops:
  6.5 94.6 %all-gather.2.cloned.1.call-start = ((), (), s32[]{:S(2)}) async-start(), calls=%async_computation.3 | async-start | bytes 6553600 | tf_op jit(solution)/shard_map/all_gather | solution.py:41
  61.5 118.4 %reduce-scatter.2.cloned.1.call-start = ((), (), s32[]{:S(2)}) async-start(), calls=%async_computation.4 | async-start | bytes 6553600 | tf_op jit(solution)/shard_map/reduce_scatter | solution.py:47
  128.6 56.9 %copy-start = (f32[256,2]{0,1:T(2,128)S(1)}, f32[256,2]{0,1:T(2,128)}, u32[]{:S(2)}) copy-start(f32[256,2]{0,1:T(2,128)} %param.10) | copy-start | bytes 6148
  180.0 36.7 %all-to-all-start.1 = ((bf16[8,160,512]{2,1,0:T(8,128)(2,1)}), bf16[8,160,512]{2,1,0:T(8,128)(2,1)S(1)}, u32[]{:S(2)}, u32[]{:S(2)}) async-start(bf16[8,160,512]{2,1,0:T(8,128)(2,1)} %bitcast.40), calls=%async_computation.2 | async-start | bytes 2621440 | tf_op jit(solution)/shard_map/all_to_all | solution.py:50
Sparse Core Ops, SparseCore 0:
  61.7 39.4 all-gather.1
  128.8 51.1 reduce-scatter.1
where the time goes:
time: 228 us
  waiting for transfers between devices  122 us (54%)
  blocking collectives  38.6 us (17%)
  matrix products  27.5 us (12%)
  between operations  13.6 us (6%)
  local copies, waits for them, and re-layouts  11.8 us (5%)
  other arithmetic  9.14 us (4%)
  starting transfers between devices  5.56 us (2%)
    reduce_scatter x1, waiting for transfers between devices, body(): lax.psum_scatter(partial_value.astype(jnp.bfloat16), 'tp', scatter_dimens...  51.3 us
    all_gather x1, waiting for transfers between devices, body(): arrived = lax.all_gather(pieces, 'tp', axis=2, tiled=True)  39.5 us
    all_to_all x1, blocking collectives, body(): lax.all_to_all(doubled, 'ep', split_axis=0, concat_axis=0, tiled=True)  38.6 us
    all_to_all x1, waiting for transfers between devices, body(): lax.all_to_all(reduced.reshape(ep_count, capacity, -1), 'ep', split_axis=...  31.1 us
    dot_general x1, matrix products, body(): jnp.dot(hidden, w_down[0], preferred_element_type=jnp.float32)  17.6 us
    dot_general x1, matrix products, body(): gate = jnp.dot(routed, w_gate[0], preferred_element_type=jnp.float32)  9.98 us
    all_to_all x1, starting transfers between devices, body(): lax.all_to_all(reduced.reshape(ep_count, capacity, -1), 'ep', split_axis=...  5.52 us
  transfers between devices with their start and end apart: 3, of which 3 were waited for; matrix products, arithmetic and copies ran while one was open for 0% of the time, Pallas kernels for 0%

commit v1 on v0

--- a/solution.py
+++ b/solution.py
@@ -38,7 +38,8 @@
     portion = lax.dynamic_slice_in_dim(outgoing, lax.axis_index("tp") * columns, columns, 2)
     doubled = jnp.repeat(portion, HALVES, axis=0)
     pieces = lax.all_to_all(doubled, "ep", split_axis=0, concat_axis=0, tiled=True)
-    arrived = lax.all_gather(pieces, "tp", axis=2, tiled=True)
+    sent = jnp.stack([pieces] * lax.axis_size("tp"))
+    arrived = jnp.concatenate(lax.all_to_all(sent, "tp", 0, 0), axis=2)
     routed = arrived.reshape(-1, width)
     gate = jnp.dot(routed, w_gate[0], preferred_element_type=jnp.float32)
     up = jnp.dot(routed, w_up[0], preferred_element_type=jnp.float32)

time: 228 us -> 255 us (1.12)
  blocking collectives: 38.6 us -> 100 us
  waiting for transfers between devices: 122 us -> 80.5 us
  local copies, waits for them, and re-layouts: 11.8 us -> 21.1 us
  matrix products: 27.5 us -> 24.7 us
    all_to_all x0 -> x1, blocking collectives: none -> 62 us  [body(): arrived = jnp.concatenate(lax.all_to_all(sent, 'tp', 0, 0), axis=2)]
    all_gather x1 -> x0, waiting for transfers between devices: 39.5 us -> none  [body(): arrived = lax.all_gather(pieces, 'tp', axis=2, tiled=True)]
    unnamed x4 -> x9, local copies, waits for them, and re-layouts: 0.94 us -> 5.56 us
    reshape x1 -> x2, local copies, waits for them, and re-layouts: 0.02 us -> 4.07 us  [the longest x1 4.05 us: body(): arrived = jnp.concatenate(lax.all_to_all(sent, 'tp', 0, 0), axis=2)]
    dot_general x1, matrix products: 9.98 us -> 7.15 us  [body(): gate = jnp.dot(routed, w_gate[0], preferred_element_type=jnp.float32)]
  transfers between devices with their start and end apart: 3 -> 2, of which waited for: 3 -> 2; matrix products, arithmetic and copies ran while one was open for 0% -> 0% of each run, Pallas kernels for 0% -> 0%
where the time goes in v1:
time: 255 us
  blocking collectives  100 us (39%)
  waiting for transfers between devices  80.5 us (32%)
  matrix products  24.7 us (10%)
  local copies, waits for them, and re-layouts  21.1 us (8%)
  between operations  13.6 us (5%)
  other arithmetic  9.14 us (4%)
  starting transfers between devices  5.53 us (2%)
    all_to_all x1, blocking collectives, body(): arrived = jnp.concatenate(lax.all_to_all(sent, 'tp', 0, 0), axis=2)  62 us
    reduce_scatter x1, waiting for transfers between devices, body(): lax.psum_scatter(partial_value.astype(jnp.bfloat16), 'tp', scatter_dimens...  49.4 us
    all_to_all x1, blocking collectives, body(): lax.all_to_all(doubled, 'ep', split_axis=0, concat_axis=0, tiled=True)  38.5 us
    all_to_all x1, waiting for transfers between devices, body(): lax.all_to_all(reduced.reshape(ep_count, capacity, -1), 'ep', split_axis=...  31.1 us
    dot_general x1, matrix products, body(): jnp.dot(hidden, w_down[0], preferred_element_type=jnp.float32)  17.5 us
    dot_general x1, matrix products, body(): gate = jnp.dot(routed, w_gate[0], preferred_element_type=jnp.float32)  7.15 us
    unnamed x9, local copies, waits for them, and re-layouts  5.56 us
    all_to_all x1, starting transfers between devices, body(): lax.all_to_all(reduced.reshape(ep_count, capacity, -1), 'ep', split_axis=...  5.52 us
  transfers between devices with their start and end apart: 2, of which 2 were waited for; matrix products, arithmetic and copies ran while one was open for 0% of the time, Pallas kernels for 0%

profile of v1, /device:TPU:0, one launch (start us, length us, event | category | flops | bytes accessed | tf_op | source)
XLA Modules:
  0.0 255.0 jit_solution(7795269746719498098)
XLA Ops:
  6.5 0.8 copy.14
  7.4 0.1 eq.27
  7.5 1.2 reduce-window.6
  8.8 0.2 slice_reduce_fusion
  9.0 0.7 broadcast_multiply_fusion
  9.7 0.2 reduce-window.9
  10.0 0.1 copy.13
  10.1 0.1 mul.64
  10.3 2.4 scatter_custom_fusion
  12.8 1.4 convert_reduce_fusion
  14.2 1.6 fusion.6
  15.9 1.6 fusion.8
  17.5 0.1 concatenate.3
  17.6 4.1 %gather_fusion = bf16[640,2048]{1,0:T(8,128)(2,1)} fusion(bf16[257,2048]{1,0:T(8,128)(2,1)S(1)} %concatenate.3, s32[1024]{0:T(1024)S(1)} %pad_clamp_fusion.1), kind=kCustom, calls=%fused_computation | custom fusion | bytes 5245440 | tf_op jit(solution)/shard_map/gather | solution.py:36
  21.7 1.1 constant_dynamic-slice_fusion
  22.8 0.1 broadcast_in_dim.8
  22.9 38.5 %all_to_all.15 = bf16[8,160,512]{2,1,0:T(8,128)(2,1)S(1)} all-to-all(bf16[8,160,512]{2,1,0:T(8,128)(2,1)S(1)} %bitcast.45), channel_id=1, replica_groups=mesh['ep'=8,'tp'=4] {'ep'}, dimensions={0} | all-to-all | bytes 2621440 | tf_op jit(solution)/shard_map/all_to_all | solution.py:40
  61.4 0.6 stack.2
  62.1 62.0 %all_to_all.16 = bf16[4,8,160,512]{3,2,1,0:T(8,128)(2,1)S(1)} all-to-all(bf16[4,8,160,512]{3,2,1,0:T(8,128)(2,1)S(1)} %stack.2), channel_id=1, replica_groups=mesh['ep'=8,'tp'=4] {'tp'}, dimensions={0} | all-to-all | bytes 10485760 | tf_op jit(solution)/shard_map/all_to_all | solution.py:42
  124.0 4.1 %copy.15 = bf16[8,160,4,512]{3,2,1,0:T(4,128)(2,1)S(1)} copy(bf16[8,160,4,512]{3,1,0,2:T(8,128)(2,1)S(1)} %bitcast.41) | data formatting | bytes 10485760 | tf_op jit(solution)/shard_map/reshape | solution.py:42
  128.1 2.3 copy.16
  130.4 2.3 copy-done
  132.7 7.1 %fusion.2 = f32[1280,896]{1,0:T(8,128)} fusion(bf16[1280,2048]{1,0:T(8,128)(2,1)S(1)} %bitcast.43, bf16[1,2048,896]{2,1,0:T(8,128)(2,1)S(1)} %copy-done.2), kind=kOutput, calls=%fused_computation.7 | convolution fusion | flops 4697620480 | bytes 13500416 | tf_op jit(solution)/shard_map/dot_general | solution.py:44
  139.9 17.5 %convolution_convert_fusion = bf16[1280,2048]{1,0:T(8,128)(2,1)} fusion(bf16[1,896,2048]{2,1,0:T(8,128)(2,1)} %param.13, f32[1280,896]{1,0:T(8,128)} %fusion.2, bf16[1280,2048]{1,0:T(8,128)(2,1)} %bitcast.44, bf16[1,2048,896]{2,1,0:T(8,128)(2,1)} %param.12), kind=kOutput, calls=%fused_computation.3 | convolution fusion | flops 9404743680 | bytes 22413312 | tf_op jit(solution)/shard_map/dot_general | solution.py:47
  157.4 49.4 %reduce-scatter.2.cloned.1.call-done = bf16[1280,512]{1,0:T(8,128)(2,1)} async-done(((bf16[1280,2048]{1,0:T(8,128)(2,1)}), bf16[1280,512]{1,0:T(8,128)(2,1)}) %reduce-scatter.2.cloned.1.call-update) | async-done | bytes 1310736 | tf_op jit(solution)/shard_map/reduce_scatter | solution.py:48
  206.8 5.5 %all-to-all-start.2 = ((bf16[8,160,512]{2,1,0:T(8,128)(2,1)}), bf16[8,160,512]{2,1,0:T(8,128)(2,1)S(1)}, u32[]{:S(2)}, u32[]{:S(2)}) async-start(bf16[8,160,512]{2,1,0:T(8,128)(2,1)} %bitcast.47), calls=%async_computation.3 | async-start | bytes 2621440 | tf_op jit(solution)/shard_map/all_to_all | solution.py:51
  212.3 0.1 copy.12
  212.5 31.1 %all-to-all-done.2 = bf16[8,160,512]{2,1,0:T(8,128)(2,1)S(1)} async-done(((bf16[8,160,512]{2,1,0:T(8,128)(2,1)}), bf16[8,160,512]{2,1,0:T(8,128)(2,1)S(1)}, u32[]{:S(2)}, u32[]{:S(2)}) %all-to-all-start.2) | async-done | bytes 1310752 | tf_op jit(solution)/shard_map/all_to_all | solution.py:51
  243.6 0.2 convert_reduce_fusion.1
  243.8 1.6 gather_fusion.1
  245.4 0.6 reshape.193
  246.1 2.1 multiply_reduce_fusion
  (21 shorter events, 0.2 us)
Async XLA Ops:
  6.5 200.3 %reduce-scatter.2.cloned.1.call-start = ((), (), s32[]{:S(2)}) async-start(), calls=%async_computation.4 | async-start | bytes 6553600 | tf_op jit(solution)/shard_map/reduce_scatter | solution.py:48
  128.1 4.6 %copy-start.2 = (bf16[1,2048,896]{2,1,0:T(8,128)(2,1)S(1)}, bf16[1,2048,896]{2,1,0:T(8,128)(2,1)}, u32[]{:S(2)}) copy-start(bf16[1,2048,896]{2,1,0:T(8,128)(2,1)} %param.11) | copy-start | bytes 11010052
  130.4 2.3 copy-start
  157.4 54.9 %copy-start.1 = (f32[256,2]{0,1:T(2,128)S(1)}, f32[256,2]{0,1:T(2,128)}, u32[]{:S(2)}) copy-start(f32[256,2]{0,1:T(2,128)} %param.10) | copy-start | bytes 6148
  206.8 36.7 %all-to-all-start.2 = ((bf16[8,160,512]{2,1,0:T(8,128)(2,1)}), bf16[8,160,512]{2,1,0:T(8,128)(2,1)S(1)}, u32[]{:S(2)}, u32[]{:S(2)}) async-start(bf16[8,160,512]{2,1,0:T(8,128)(2,1)} %bitcast.47), calls=%async_computation.3 | async-start | bytes 2621440 | tf_op jit(solution)/shard_map/all_to_all | solution.py:51
Sparse Core Ops, SparseCore 0:
  157.5 49.2 reduce-scatter.1
